TPU v7x, 32 devices: a whole 2x2x4 slice. The times are simulated.
32 devices in a mesh: sp: 4 (over y, core), dp: 8 (over z, x).
Axes of the slice: x: 2, y: 2, z: 4, core: 2. Of those that a mesh axis runs over, the one named last changes fastest.
Arguments:
- queries: bfloat16 [8, 704, 2048], P('dp', 'sp'), may hold values from -24 to 24, as said below
- keys: bfloat16 [8, 704, 256], P('dp', 'sp'), may hold values from -24 to 24, as said below
- tokens: bfloat16 [8, 704, 2304], P('dp', 'sp'), may hold values from -18 to 18
- w_value: bfloat16 [2304, 256], P('dp'), may hold values from -0.125 to 0.125
- q_gain: float32 [128], replicated, may hold values from 0.5 to 6, as said below
- k_gain: float32 [128], replicated, may hold values from 0.5 to 6, as said below
Outputs:
- attended: bfloat16 [8, 704, 2048], P('dp', 'sp')
Inputs may be any that keep to these rules, and one draw needn't show every extreme that they name: `queries`: real-valued projected query entries. `keys`: real-valued projected key entries. `q_gain`: positive gains. `k_gain`: positive gains.
All inputs are finite; a program needn't handle non-finite values.
Results may differ from a plain program's by a relative error of at most 0.0022.
The roundings to bfloat16 on the way count: a program that leaves them out, or rounds other values in their place, can miss the bound.
Values may be sent and summed in bfloat16 or wider, within the bound.
A program may use at most 64 MiB of HBM per device.

v0:
```python
import math
import jax
import jax.numpy as jnp
from jax import lax
from jax.sharding import PartitionSpec as P

HD = 128
QH = 16
KVH = 2
GRID_W = 64
epsilon = 1e-06


def unit_rms(vectors, scaling):
    return (
        vectors * lax.rsqrt(jnp.mean(vectors * vectors, axis=-1, keepdims=True) + epsilon) * scaling
    )


def rotary(vectors, row_pos, col_pos):
    head_width = vectors.shape[-1]
    half_width = head_width // 2
    quarter = half_width // 2
    frequency = 10000.0 ** (-jnp.arange(quarter, dtype=jnp.float32) * 2.0 / half_width)

    def rotate_half(section, angle_pos):
        angles = angle_pos[:, None, None] * frequency
        cosine = jnp.cos(angles)
        sine_table = jnp.sin(angles)
        leading = section[..., :quarter]
        second = section[..., quarter:]
        return jnp.concatenate(
            [leading * cosine - second * sine_table, second * cosine + leading * sine_table],
            axis=-1,
        )

    return jnp.concatenate(
        [
            rotate_half(vectors[..., :half_width], row_pos),
            rotate_half(vectors[..., half_width:], col_pos),
        ],
        axis=-1,
    )


def attend(query_heads, key_heads, value_heads):
    length, item_count, joined = query_heads.shape
    head_width = key_heads.shape[-1]
    per_copy = joined // head_width
    block_rows = math.gcd(length, 512)
    blocked = query_heads.reshape(
        length // block_rows, block_rows, item_count, per_copy, head_width
    )

    def one_block(query_block):
        scores = jnp.einsum(
            "qnad,knd->naqk", query_block, key_heads, preferred_element_type=jnp.float32
        ) * head_width ** (-0.5)
        highest = jnp.max(scores, axis=-1, keepdims=True)
        weights = jnp.exp(scores - highest)
        probability = (weights / jnp.sum(weights, axis=-1, keepdims=True)).astype(jnp.bfloat16)
        blended = jnp.einsum(
            "naqk,knd->qnad", probability, value_heads, preferred_element_type=jnp.float32
        )
        return blended.astype(jnp.bfloat16).reshape(block_rows, item_count, joined)

    return lax.map(one_block, blocked).reshape(length, item_count, joined)


def per_device(queries, keys, tokens, w_value, q_gain, k_gain):
    tok_rows = tokens.shape[1]
    devices_sp = lax.axis_size("sp")
    copies = max(devices_sp, KVH)
    repeat_count = copies // KVH
    local_copies = copies // devices_sp
    joined = QH // copies * HD
    token_rows = tokens[0]
    value_sum = jnp.dot(
        token_rows,
        lax.all_gather(w_value, "dp", axis=0, tiled=True),
        preferred_element_type=jnp.float32,
    )
    values = value_sum.astype(jnp.bfloat16).reshape(tok_rows, KVH, HD)
    sp_index = lax.axis_index("sp")
    positions = sp_index * tok_rows + jnp.arange(tok_rows, dtype=jnp.int32)
    row_pos = (positions // GRID_W).astype(jnp.float32)
    col_pos = (positions % GRID_W).astype(jnp.float32)
    query_norm = unit_rms(queries[0].astype(jnp.float32).reshape(tok_rows, QH, HD), q_gain)
    query_rot = rotary(query_norm, row_pos, col_pos).astype(jnp.bfloat16)
    key_norm = unit_rms(keys[0].astype(jnp.float32).reshape(tok_rows, KVH, HD), k_gain)
    key_rot = rotary(key_norm, row_pos, col_pos).astype(jnp.bfloat16)
    query_grouped = query_rot.reshape(tok_rows, copies, joined)
    query_local = lax.all_to_all(query_grouped, "sp", split_axis=1, concat_axis=0, tiled=True)
    key_all, value_all = (
        lax.all_gather(key_rot, "sp", axis=0, tiled=True),
        lax.all_gather(values, "sp", axis=0, tiled=True),
    )
    kv_count = max(1, local_copies // repeat_count)
    kv_start = sp_index * local_copies // repeat_count
    key_local = lax.dynamic_slice_in_dim(key_all, kv_start, kv_count, 1)
    value_local = lax.dynamic_slice_in_dim(value_all, kv_start, kv_count, 1)
    attended = attend(query_local, key_local, value_local)
    returned = lax.all_to_all(attended, "sp", split_axis=0, concat_axis=1, tiled=True)
    return returned.reshape(1, tok_rows, QH * HD)


def solution(mesh):
    in_specs = (
        P("dp", "sp", None),
        P("dp", "sp", None),
        P("dp", "sp", None),
        P("dp", None),
        P(),
        P(),
    )
    out_specs = P("dp", "sp", None)
    return jax.shard_map(
        per_device, mesh=mesh, in_specs=in_specs, out_specs=out_specs, check_vma=False
    )
```

profile of v0, /device:TPU:0, one launch (start us, length us, event | category | flops | bytes accessed | tf_op | source)
XLA Modules:
  0.0 100.0 jit_solution(4973666312808731522)
XLA Ops:
  6.5 0.7 all-gather.2.cloned.1.call-update
  7.3 1.3 %convert_bitcast_fusion = f32[22,8,16,128]{3,1,2,0:T(8,128)S(1)} fusion(bf16[1,176,2048]{2,1,0:T(8,128)(2,1)} %param.8), kind=kLoop, calls=%fused_computation.13 | loop fusion | flops 360448 | bytes 2162688
  8.8 0.4 multiply_reduce_fusion
  9.4 0.7 multiply_cosine_fusion.1
  10.2 0.4 multiply_multiply_fusion
  10.6 1.2 %subtract_convert_fusion.1 = (bf16[176,16,32]{2,1,0:T(8,128)(2,1)S(1)}, bf16[176,16,32]{2,1,0:T(8,128)(2,1)S(1)}, bf16[176,16,32]{2,1,0:T(8,128)(2,1)S(1)}, bf16[176,16,32]{2,1,0:T(8,128)(2,1)S(1)}) fusion(f32[176,16,128]{2,1,0:T(8,128)S(1)} %multiply_multiply_fusion, f32[176,32]{1,0:T(8,128)S(1)} %get-tuple-element.83, f32[176,32]{1,0:T(8,128)S(1)} %get-tuple-element.82, ...), kind=kLoop, calls=%fused_computation.17 | loop fusion | flops 1441792 | bytes 2252800 | tf_op jit(solution)/shard_map/convert.6
  11.8 0.9 pad_maximum_fusion
  13.1 1.0 copy.37
  14.1 4.4 %all-to-all-start = ((bf16[176,4,512]{2,0,1:T(8,128)(2,1)}), bf16[176,4,512]{2,0,1:T(8,128)(2,1)S(1)}, u32[]{:S(2)}, u32[]{:S(2)}) async-start(bf16[176,4,512]{2,0,1:T(8,128)(2,1)} %copy.37), calls=%async_computation | async-start | bytes 1441792 | tf_op jit(solution)/shard_map/all_to_all | solution.py:93
  19.1 0.6 subtract_convert_fusion.3
  19.8 0.6 pad_maximum_fusion.1
  20.3 11.8 %all_gather.9 = bf16[704,2,128]{2,1,0:T(2,128)(2,1)S(1)} all-gather(bf16[176,2,128]{2,1,0:T(2,128)(2,1)S(1)} %pad_maximum_fusion.1), channel_id=1, replica_groups=mesh['sp'=4,'dp'=8] {'sp'}, dimensions={0}, use_global_device_ids=true | all-gather | bytes 450560 | tf_op jit(solution)/shard_map/all_gather | solution.py:95
  32.8 20.6 %all-gather.2.cloned.1.call-done = bf16[2304,256]{1,0:T(8,128)(2,1)} async-done(((bf16[288,256]{1,0:T(8,128)(2,1)}), bf16[2304,256]{1,0:T(8,128)(2,1)}) %all-gather.2.cloned.1.call-update) | async-done | bytes 1179664 | tf_op jit(solution)/shard_map/all_gather | solution.py:80
  53.3 1.7 %fusion.6 = bf16[22,2,8,128]{3,2,1,0:T(8,128)(2,1)S(1)} fusion(bf16[2304,256]{1,0:T(8,128)(2,1)} %all-gather.2.cloned.1.call-done, bf16[1,176,2304]{2,1,0:T(8,128)(2,1)S(1)} %copy-done), kind=kOutput, calls=%fused_computation.21 | convolution fusion | flops 207663104 | bytes 2080768 | tf_op jit(solution)/shard_map/dot_general | solution.py:78
  55.0 6.3 %all_gather.11 = bf16[704,2,128]{2,0,1:T(8,128)(2,1)S(1)} all-gather(bf16[176,2,128]{2,0,1:T(8,128)(2,1)S(1)} %bitcast.73), channel_id=1, replica_groups=mesh['sp'=4,'dp'=8] {'sp'}, dimensions={0}, use_global_device_ids=true | all-gather | bytes 450560 | tf_op jit(solution)/shard_map/all_gather | solution.py:96
  61.3 13.4 %while.10 = (s32[]{:T(128)}, bf16[11,64,1,512]{3,1,2,0:T(8,128)(2,1)S(1)}, bf16[11,64,1,4,128]{4,3,1,0,2:T(4,128)(2,1)S(1)}, bf16[704,1,128]{2,0,1:T(8,128)(2,1)...) while((s32[]{:T(128)}, bf16[11,64,1,512]{3,1,2,0:T(8,128)(2,1)S(1)}, ...), condition=%wide.region_5.6_spmd, body=%wide.region_2.5_spmd.sunk | while | flops 93568512 | bytes 3183693 | solution.py:67
  63.2 0.4 fusion.22
  74.7 0.5 broadcast.195
  75.2 1.2 %reduce.2 = bf16[704,512]{1,0:T(8,128)(2,1)S(1)} reduce(bf16[704,1,512]{2,0,1:T(8,128)(2,1)S(1)} %bitcast.72, bf16[]{:T(256)} %broadcast.195), dimensions={1}, to_apply=%copy.43.reduce_sub_computation | reduce | bytes 1441794 | tf_op jit(solution)/shard_map/reshape | solution.py:67
  76.4 0.6 reshape.235
  77.0 13.3 %all_to_all.30 = bf16[4,2,45056]{2,1,0:T(2,128)(2,1)S(1)} all-to-all(bf16[4,2,45056]{2,1,0:T(2,128)(2,1)S(1)} %reshape.235), channel_id=1, replica_groups=mesh['sp'=4,'dp'=8] {'sp'}, dimensions={0} | all-to-all | bytes 1441792 | tf_op jit(solution)/shard_map/all_to_all | solution.py:103
  90.3 0.7 reshape.236
  91.2 0.6 copy.44
  91.8 1.4 %reshape.230 = bf16[1,176,2048]{2,1,0:T(8,128)(2,1)} reshape(bf16[176,4,1,512]{3,1,0,2:T(4,128)(2,1)S(1)} %copy.44) | data formatting | bytes 1441792 | tf_op jit(solution)/shard_map/reshape | solution.py:104
  (104 shorter events, 14.6 us)
Async XLA Ops:
  6.5 46.8 %copy-start = (bf16[1,176,2304]{2,1,0:T(8,128)(2,1)S(1)}, bf16[1,176,2304]{2,1,0:T(8,128)(2,1)}, u32[]{:S(2)}) copy-start(bf16[1,176,2304]{2,1,0:T(8,128)(2,1)} %param.10) | copy-start | bytes 2433028
  6.5 46.8 %all-gather.2.cloned.1.call-start = ((), (), s32[]{:S(2)}) async-start(), calls=%async_computation.2 | async-start | bytes 1327104 | tf_op jit(solution)/shard_map/all_gather | solution.py:80
  8.8 1.4 %copy-start.2 = (f32[128]{0:T(128)S(1)}, f32[128]{0:T(128)}, u32[]{:S(2)}) copy-start(f32[128]{0:T(128)} %param.12) | copy-start | bytes 1540
  13.1 5.4 %copy-start.1 = (bf16[1,176,256]{2,1,0:T(8,128)(2,1)S(1)}, bf16[1,176,256]{2,1,0:T(8,128)(2,1)}, u32[]{:S(2)}) copy-start(bf16[1,176,256]{2,1,0:T(8,128)(2,1)} %param.9) | copy-start | bytes 270340
  14.1 4.8 %copy-start.3 = (f32[128]{0:T(128)S(1)}, f32[128]{0:T(128)}, u32[]{:S(2)}) copy-start(f32[128]{0:T(128)} %param.13) | copy-start | bytes 1540
  14.1 18.5 %all-to-all-start = ((bf16[176,4,512]{2,0,1:T(8,128)(2,1)}), bf16[176,4,512]{2,0,1:T(8,128)(2,1)S(1)}, u32[]{:S(2)}, u32[]{:S(2)}) async-start(bf16[176,4,512]{2,0,1:T(8,128)(2,1)} %copy.37), calls=%async_computation | async-start | bytes 1441792 | tf_op jit(solution)/shard_map/all_to_all | solution.py:93
Sparse Core Ops, SparseCore 0:
  9.5 43.7 all-gather.1
where the time goes:
time: 100 us
  blocking collectives  31.4 us (31%)
  waiting for transfers between devices  21.3 us (21%)
  between operations  13.6 us (14%)
  other arithmetic  11 us (11%)
  matrix products  10 us (10%)
  local copies, waits for them, and re-layouts  7.71 us (8%)
  starting transfers between devices  4.4 us (4%)
    all_gather x1, waiting for transfers between devices, per_device(): lax.all_gather(w_value, 'dp', axis=0, tiled=True)  20.6 us
    all_to_all x1, blocking collectives, per_device(): lax.all_to_all(attended, 'sp', split_axis=0, concat_axis=1, tiled=True)  13.3 us
    all_gather x1, blocking collectives, per_device(): lax.all_gather(key_rot, 'sp', axis=0, tiled=True)  11.8 us
    all_gather x1, blocking collectives, per_device(): lax.all_gather(values, 'sp', axis=0, tiled=True)  6.26 us
    dot_general x11, matrix products, one_block(): jnp.einsum('naqk,knd->qnad', probability, value_heads, preferred_element_...  4.43 us
    all_to_all x1, starting transfers between devices, per_device(): lax.all_to_all(query_grouped, 'sp', split_axis=1, concat_axis=0, tiled=True)  4.4 us
    dot_general x11, matrix products, one_block(): jnp.einsum('qnad,knd->naqk', query_block, key_heads, preferred_element_ty...  3.96 us
    reduce_sum x11, other arithmetic, one_block(): jnp.sum(weights, axis=-1, keepdims=True)  3.07 us
  transfers between devices with their start and end apart: 2, of which 1 were waited for; matrix products, arithmetic and copies ran while one was open for 9% of the time, Pallas kernels for 0%

commit v1 on v0

--- a/solution.py
+++ b/solution.py
@@ -100,7 +100,10 @@
     key_local = lax.dynamic_slice_in_dim(key_all, kv_start, kv_count, 1)
     value_local = lax.dynamic_slice_in_dim(value_all, kv_start, kv_count, 1)
     attended = attend(query_local, key_local, value_local)
-    returned = lax.all_to_all(attended, "sp", split_axis=0, concat_axis=1, tiled=True)
+    devices = lax.axis_size("sp")
+    blocks = jnp.stack(jnp.split(attended, devices, axis=0), axis=0)
+    blocks = lax.all_to_all(blocks, "sp", split_axis=0, concat_axis=0)
+    returned = jnp.concatenate(blocks, axis=1)
     return returned.reshape(1, tok_rows, QH * HD)
 
 

time: 100 us -> 97.3 us (0.973)
  local copies, waits for them, and re-layouts: 7.71 us -> 5.79 us
  other arithmetic: 11 us -> 9.92 us
    unnamed x12 -> x9, local copies, waits for them, and re-layouts: 1.73 us -> 0.28 us
    another operation x0 -> x2, local copies, waits for them, and re-layouts: none -> 1.44 us  [the longest x1 1.39 us: per_device(): return returned.reshape(1, tok_rows, QH * HD)]
    reshape x2 -> x1, local copies, waits for them, and re-layouts: 1.9 us -> 0.56 us  [per_device(): returned = jnp.concatenate(blocks, axis=1)]
    reshape x1 -> x0, other arithmetic: 1.19 us -> none  [attend(): return lax.map(one_block, blocked).reshape(length, item_count, joined)]
where the time goes in v1:
time: 97.3 us; the launch traced here: 97 us
  blocking collectives  31.4 us (32%)
  waiting for transfers between devices  21.3 us (22%)
  between operations  13.6 us (14%)
  matrix products  10 us (10%)
  other arithmetic  9.92 us (10%)
  local copies, waits for them, and re-layouts  5.79 us (6%)
  starting transfers between devices  4.4 us (5%)
    all_gather x1, waiting for transfers between devices, per_device(): lax.all_gather(w_value, 'dp', axis=0, tiled=True)  20.6 us
    all_to_all x1, blocking collectives, per_device(): blocks = lax.all_to_all(blocks, 'sp', split_axis=0, concat_axis=0)  13.3 us
    all_gather x1, blocking collectives, per_device(): lax.all_gather(key_rot, 'sp', axis=0, tiled=True)  11.8 us
    all_gather x1, blocking collectives, per_device(): lax.all_gather(values, 'sp', axis=0, tiled=True)  6.26 us
    dot_general x11, matrix products, one_block(): jnp.einsum('naqk,knd->qnad', probability, value_heads, preferred_element_...  4.43 us
    all_to_all x1, starting transfers between devices, per_device(): lax.all_to_all(query_grouped, 'sp', split_axis=1, concat_axis=0, tiled=True)  4.4 us
    dot_general x11, matrix products, one_block(): jnp.einsum('qnad,knd->naqk', query_block, key_heads, preferred_element_ty...  3.96 us
    reduce_sum x11, other arithmetic, one_block(): jnp.sum(weights, axis=-1, keepdims=True)  3.07 us
  transfers between devices with their start and end apart: 2, of which 1 were waited for; matrix products, arithmetic and copies ran while one was open for 9% of the time, Pallas kernels for 0%

profile of v1, /device:TPU:0, one launch (start us, length us, event | category | flops | bytes accessed | tf_op | source)
XLA Modules:
  0.0 97.0 jit_solution(7012689947114905107)
XLA Ops:
  6.5 0.7 all-gather.2.cloned.1.call-update
  7.3 1.3 %convert_bitcast_fusion = f32[22,8,16,128]{3,1,2,0:T(8,128)S(1)} fusion(bf16[1,176,2048]{2,1,0:T(8,128)(2,1)} %param.8), kind=kLoop, calls=%fused_computation.13 | loop fusion | flops 360448 | bytes 2162688
  8.8 0.4 multiply_reduce_fusion
  9.4 0.7 multiply_cosine_fusion.1
  10.2 0.4 multiply_multiply_fusion
  10.6 1.2 %subtract_convert_fusion.1 = (bf16[176,16,32]{2,1,0:T(8,128)(2,1)S(1)}, bf16[176,16,32]{2,1,0:T(8,128)(2,1)S(1)}, bf16[176,16,32]{2,1,0:T(8,128)(2,1)S(1)}, bf16[176,16,32]{2,1,0:T(8,128)(2,1)S(1)}) fusion(f32[176,16,128]{2,1,0:T(8,128)S(1)} %multiply_multiply_fusion, f32[176,32]{1,0:T(8,128)S(1)} %get-tuple-element.87, f32[176,32]{1,0:T(8,128)S(1)} %get-tuple-element.86, ...), kind=kLoop, calls=%fused_computation.17 | loop fusion | flops 1441792 | bytes 2252800 | tf_op jit(solution)/shard_map/convert.6
  11.8 0.9 pad_maximum_fusion
  13.1 1.0 %copy.38 = bf16[176,4,512]{2,0,1:T(8,128)(2,1)} copy(bf16[176,4,512]{2,1,0:T(4,128)(2,1)S(1)} %convert_element_type.64) | data formatting | bytes 1441792 | tf_op jit(solution)/shard_map/convert_element_type | solution.py:89
  14.1 4.4 %all-to-all-start = ((bf16[176,4,512]{2,0,1:T(8,128)(2,1)}), bf16[176,4,512]{2,0,1:T(8,128)(2,1)S(1)}, u32[]{:S(2)}, u32[]{:S(2)}) async-start(bf16[176,4,512]{2,0,1:T(8,128)(2,1)} %copy.38), calls=%async_computation | async-start | bytes 1441792 | tf_op jit(solution)/shard_map/all_to_all | solution.py:93
  19.1 0.6 subtract_convert_fusion.3
  19.8 0.6 pad_maximum_fusion.2
  20.3 11.8 %all_gather.9 = bf16[704,2,128]{2,1,0:T(2,128)(2,1)S(1)} all-gather(bf16[176,2,128]{2,1,0:T(2,128)(2,1)S(1)} %pad_maximum_fusion.2), channel_id=1, replica_groups=mesh['sp'=4,'dp'=8] {'sp'}, dimensions={0}, use_global_device_ids=true | all-gather | bytes 450560 | tf_op jit(solution)/shard_map/all_gather | solution.py:95
  32.8 20.6 %all-gather.2.cloned.1.call-done = bf16[2304,256]{1,0:T(8,128)(2,1)} async-done(((bf16[288,256]{1,0:T(8,128)(2,1)}), bf16[2304,256]{1,0:T(8,128)(2,1)}) %all-gather.2.cloned.1.call-update) | async-done | bytes 1179664 | tf_op jit(solution)/shard_map/all_gather | solution.py:80
  53.3 1.7 %fusion.6 = bf16[22,2,8,128]{3,2,1,0:T(8,128)(2,1)S(1)} fusion(bf16[2304,256]{1,0:T(8,128)(2,1)} %all-gather.2.cloned.1.call-done, bf16[1,176,2304]{2,1,0:T(8,128)(2,1)S(1)} %copy-done), kind=kOutput, calls=%fused_computation.21 | convolution fusion | flops 207663104 | bytes 2080768 | tf_op jit(solution)/shard_map/dot_general | solution.py:78
  55.0 6.3 %all_gather.11 = bf16[704,2,128]{2,0,1:T(8,128)(2,1)S(1)} all-gather(bf16[176,2,128]{2,0,1:T(8,128)(2,1)S(1)} %bitcast.79), channel_id=1, replica_groups=mesh['sp'=4,'dp'=8] {'sp'}, dimensions={0}, use_global_device_ids=true | all-gather | bytes 450560 | tf_op jit(solution)/shard_map/all_gather | solution.py:96
  61.3 13.4 %while.10 = (s32[]{:T(128)}, bf16[11,64,1,512]{3,1,2,0:T(8,128)(2,1)S(1)}, bf16[11,64,1,4,128]{4,3,1,0,2:T(4,128)(2,1)S(1)}, bf16[704,1,128]{2,0,1:T(8,128)(2,1)...) while((s32[]{:T(128)}, bf16[11,64,1,512]{3,1,2,0:T(8,128)(2,1)S(1)}, ...), condition=%wide.region_5.6_spmd, body=%wide.region_2.5_spmd.sunk | while | flops 93568512 | bytes 3183693 | solution.py:67
  63.2 0.4 fusion.22
  64.4 0.4 fusion.22
  66.9 0.4 fusion.22
  68.1 0.4 fusion.22
  70.5 0.4 fusion.22
  74.9 13.3 %all_to_all.20 = bf16[4,176,1,512]{3,1,2,0:T(8,128)(2,1)S(1)} all-to-all(bf16[4,176,1,512]{3,1,2,0:T(8,128)(2,1)S(1)} %pad_maximum_fusion.1), channel_id=1, replica_groups=mesh['sp'=4,'dp'=8] {'sp'}, dimensions={0} | all-to-all | bytes 1441792 | tf_op jit(solution)/shard_map/all_to_all | solution.py:105
  88.2 0.6 copy.44
  88.8 1.4 %reshape_reshape.3 = bf16[1,176,2048]{2,1,0:T(8,128)(2,1)} reshape(bf16[176,4,1,512]{3,1,0,2:T(4,128)(2,1)S(1)} %copy.44) | data formatting | bytes 1441792 | tf_op jit(solution)/shard_map/reshape;reshape | solution.py:107
  (101 shorter events, 13.0 us)
Async XLA Ops:
  6.5 46.8 %copy-start = (bf16[1,176,2304]{2,1,0:T(8,128)(2,1)S(1)}, bf16[1,176,2304]{2,1,0:T(8,128)(2,1)}, u32[]{:S(2)}) copy-start(bf16[1,176,2304]{2,1,0:T(8,128)(2,1)} %param.10) | copy-start | bytes 2433028
  6.5 46.8 %all-gather.2.cloned.1.call-start = ((), (), s32[]{:S(2)}) async-start(), calls=%async_computation.2 | async-start | bytes 1327104 | tf_op jit(solution)/shard_map/all_gather | solution.py:80
  8.8 1.4 %copy-start.2 = (f32[128]{0:T(128)S(1)}, f32[128]{0:T(128)}, u32[]{:S(2)}) copy-start(f32[128]{0:T(128)} %param.12) | copy-start | bytes 1540
  13.1 5.4 %copy-start.1 = (bf16[1,176,256]{2,1,0:T(8,128)(2,1)S(1)}, bf16[1,176,256]{2,1,0:T(8,128)(2,1)}, u32[]{:S(2)}) copy-start(bf16[1,176,256]{2,1,0:T(8,128)(2,1)} %param.9) | copy-start | bytes 270340
  14.1 4.8 %copy-start.3 = (f32[128]{0:T(128)S(1)}, f32[128]{0:T(128)}, u32[]{:S(2)}) copy-start(f32[128]{0:T(128)} %param.13) | copy-start | bytes 1540
  14.1 18.5 %all-to-all-start = ((bf16[176,4,512]{2,0,1:T(8,128)(2,1)}), bf16[176,4,512]{2,0,1:T(8,128)(2,1)S(1)}, u32[]{:S(2)}, u32[]{:S(2)}) async-start(bf16[176,4,512]{2,0,1:T(8,128)(2,1)} %copy.38), calls=%async_computation | async-start | bytes 1441792 | tf_op jit(solution)/shard_map/all_to_all | solution.py:93
Sparse Core Ops, SparseCore 0:
  9.5 43.7 all-gather.1
